TPU v7x, 32 devices: a whole 2x2x4 slice. The times are simulated.
32 devices in a mesh: sp: 4 (over y, x), tp: 8 (over z, core).
Axes of the slice: x: 2, y: 2, z: 4, core: 2. Of those that a mesh axis runs over, the one named last changes fastest.
Arguments:
- queries: bfloat16 [4096, 2048], P('sp', 'tp'), may hold values from -8 to 8
- keys: bfloat16 [4096, 512], P('sp'), may hold values from -6 to 6
- values: bfloat16 [4096, 512], P('sp'), may hold values from -6 to 6
- query_gain: float32 [2048], P('tp'), may hold values from 0.2 to 40
- key_gain: float32 [128], replicated, may hold values from 0.1 to 1.9
- out_weight: bfloat16 [2048, 2048], replicated, may hold values from -0.125 to 0.125
- residual: bfloat16 [4096, 2048], P(('sp', 'tp')), may hold values from -2 to 2
- norm_gain: float32 [2048], replicated, may hold values from 0.1 to 1.9
- route_experts: int32 [4096, 2], P(('sp', 'tp')), may hold values from 0 to 3, as said below
- expert_scores: float32 [4096, 2], P(('sp', 'tp')), may hold values from -9 to 9
- group_prob: float32 [4096], P(('sp', 'tp')), may hold values from 0.5 to 1
- w_gate: bfloat16 [4, 2048, 2048], P('sp', None, 'tp'), may hold values from -0.125 to 0.125
- w_up: bfloat16 [4, 2048, 2048], P('sp', None, 'tp'), may hold values from -0.125 to 0.125
- w_down: bfloat16 [4, 2048, 2048], P('sp', 'tp'), may hold values from -0.125 to 0.125
Outputs:
- mixed: bfloat16 [4096, 2048], P(('sp', 'tp'))
Inputs may be any that keep to these rules, and one draw needn't show every extreme that they name: `route_experts`: each row names 2 different experts of one group, expert e lying in group e // 2. In the rows of one device (aligned blocks of 128 rows) 5 * 16 rows choose one group and the others another; inside a group those rows are spread over its experts as evenly as whole numbers allow, so no expert is named by more than 80 rows of one device and some expert by exactly 80.
All inputs are finite; a program needn't handle non-finite values.
Results may differ from a plain program's by a relative error of at most 0.025.
Values may be sent and summed in bfloat16 or wider, within the bound.
A program may use at most 128 MiB of HBM per device.

v0:
```python
import functools

import jax
import jax.numpy as jnp
from jax import lax
from jax.experimental import pallas as pl
from jax.experimental.pallas import tpu as pltpu
from jax.sharding import PartitionSpec as P


GROUPS = 2
GRID_W = 64

rope_base = 10000.0
norm_eps = 1e-06
LOG2E = 1.4426950408889634


def rope_tables(first_token, span_tokens, head_size):
    lane = jnp.arange(head_size, dtype=jnp.int32)
    half, quarter = head_size // 2, head_size // 4
    index = (lane // 2) % quarter
    frequency = rope_base ** (-index.astype(jnp.float32) * 4.0 / head_size)
    sign = jnp.where(lane % 2 == 0, -1.0, 1.0).astype(jnp.float32)
    rows = (first_token // GRID_W + jnp.arange(span_tokens // GRID_W, dtype=jnp.int32)).astype(
        jnp.float32
    )
    columns = jnp.arange(GRID_W, dtype=jnp.float32)
    angles = jnp.concatenate([rows, columns])[:, None] * frequency[None, :]
    cosines, sines = lax.optimization_barrier((jnp.cos(angles), jnp.sin(angles) * sign[None, :]))

    def spread(table):
        row_part = table[: rows.shape[0]][:, None, :]
        column_part = table[rows.shape[0] :][None, :, :]
        return jnp.where(lane[None, None, :] < half, row_part, column_part).reshape(
            span_tokens, head_size
        )

    return spread(cosines), spread(sines)


def norm_turn(raw, gain, cosines, sines):
    wide = raw.astype(jnp.float32)
    size = wide.shape[1]
    factor = lax.rsqrt(jnp.mean(wide * wide, axis=1, keepdims=True) + norm_eps)
    scaled = wide * factor * gain
    lane = lax.broadcasted_iota(jnp.int32, scaled.shape, 1)
    swapped = jnp.where(
        lane % 2 == 0, pltpu.roll(scaled, size - 1, 1), pltpu.roll(scaled, 1, 1)
    )
    return (scaled * cosines + swapped * sines).astype(jnp.bfloat16)


def prep_kernel(place_ref, key_ref, value_ref, cos_ref, sin_ref, gain_ref, out_ref):
    size = key_ref.shape[1]
    out_ref[:, :size] = norm_turn(key_ref[...], gain_ref[...], cos_ref[...], sin_ref[...])
    out_ref[:, size:] = value_ref[...]


def prep_keys(keys, values, key_gain, cosines, sines, place, parts):
    size = cosines.shape[1]
    span = cosines.shape[0] // parts
    block = min(span, 512)
    steps = span // block
    spec = pltpu.PrefetchScalarGridSpec(
        num_scalar_prefetch=1,
        grid=(steps,),
        in_specs=[
            pl.BlockSpec((block, size), lambda i, h: (i + h[1] * steps, h[0])),
            pl.BlockSpec((block, size), lambda i, h: (i + h[1] * steps, h[0])),
            pl.BlockSpec((block, size), lambda i, h: (i + h[1] * steps, 0)),
            pl.BlockSpec((block, size), lambda i, h: (i + h[1] * steps, 0)),
            pl.BlockSpec((1, size), lambda i, h: (0, 0)),
        ],
        out_specs=pl.BlockSpec((block, 2 * size), lambda i, h: (i, 0)),
    )
    return pl.pallas_call(
        prep_kernel,
        grid_spec=spec,
        out_shape=jax.ShapeDtypeStruct((span, 2 * size), jnp.bfloat16),
        cost_estimate=pl.CostEstimate(flops=span * size * 16, bytes_accessed=span * size * 16, transcendentals=0),
        name="prep_keys",
    )(place, keys, values, cosines, sines, key_gain.reshape(1, size))


def attend_kernel(count, chunk, q_ref, cos_ref, sin_ref, gain_ref, *rest):
    kv_refs, out_ref, wide_values = rest[:count], rest[count], rest[count + 1]
    size = q_ref.shape[1]
    span = kv_refs[0].shape[0]

    @pl.when((pl.program_id(0) == 0) & (pl.program_id(1) == 0))
    def _():
        for n, kv in enumerate(kv_refs):
            wide_values[n * span : (n + 1) * span, :size] = kv[:, size:]
        wide_values[:, size:] = jnp.ones((wide_values.shape[0], size), jnp.bfloat16)

    query = norm_turn(q_ref[...], gain_ref[...], cos_ref[...], sin_ref[...])
    scores = []
    for kv in kv_refs:
        for start in range(0, span, chunk):
            scores.append(
                lax.dot_general(
                    query,
                    kv[start : start + chunk, :size],
                    (((1,), (1,)), ((), ())),
                    preferred_element_type=jnp.float32,
                )
            )
    top = functools.reduce(jnp.maximum, [jnp.max(s, axis=1, keepdims=True) for s in scores])
    factor = size ** (-0.5) * LOG2E
    total = None
    for n, s in enumerate(scores):
        raised = jnp.exp2((s - top) * factor).astype(jnp.bfloat16)
        part = jnp.dot(
            raised,
            wide_values[n * chunk : (n + 1) * chunk, :],
            preferred_element_type=jnp.float32,
        )
        total = part if total is None else total + part
    out_ref[...] = (total[:, :size] / total[:, size:]).astype(jnp.bfloat16)


def attend(queries, query_gain, cosines, sines, pieces):
    span, size = cosines.shape
    local_heads = queries.shape[1] // size
    piece_rows = pieces[0].shape[0]
    key_total = piece_rows * len(pieces)
    block = min(span, max(8, (1 << 20) // key_total))
    chunk = min(piece_rows, 1024)
    whole = pl.BlockSpec((piece_rows, 2 * size), lambda h, i: (0, 0))
    return pl.pallas_call(
        functools.partial(attend_kernel, len(pieces), chunk),
        grid=(local_heads, span // block),
        in_specs=[
            pl.BlockSpec((block, size), lambda h, i: (i, h)),
            pl.BlockSpec((block, size), lambda h, i: (i, 0)),
            pl.BlockSpec((block, size), lambda h, i: (i, 0)),
            pl.BlockSpec((1, size), lambda h, i: (0, h)),
        ]
        + [whole] * len(pieces),
        out_specs=pl.BlockSpec((block, size), lambda h, i: (i, h)),
        out_shape=jax.ShapeDtypeStruct(queries.shape, jnp.bfloat16),
        scratch_shapes=[pltpu.VMEM((key_total, 2 * size), jnp.bfloat16)],
        compiler_params=pltpu.CompilerParams(vmem_limit_bytes=56 * 1024 * 1024),
        cost_estimate=pl.CostEstimate(
            flops=8 * span * local_heads * key_total * size,
            bytes_accessed=4 * key_total * size * 2,
            transcendentals=span * local_heads * key_total,
        ),
        name="attend",
    )(queries, cosines, sines, query_gain.reshape(1, -1), *pieces)


def routed_general(normed, route_experts, w_gate, w_up, w_down, mixing):
    row_count, model_width = normed.shape
    seq_size = lax.axis_size("sp")
    local_experts = w_gate.shape[0]
    expert_total = local_experts * seq_size
    group_experts = expert_total // GROUPS
    top_count = route_experts.shape[1]
    capacity = (top_count * (5 * row_count // 8) + group_experts - 1) // group_experts
    chosen_flat = route_experts.reshape(-1)
    expert_ids = jnp.arange(expert_total, dtype=jnp.int32)
    onehot = (chosen_flat[:, None] == expert_ids[None, :]).astype(jnp.int32)
    ordinal = jnp.sum((jnp.cumsum(onehot, axis=0) - onehot) * onehot, axis=1)
    slot_of = chosen_flat * capacity + ordinal
    slot_ids = jnp.arange(expert_total * capacity, dtype=jnp.int32)
    placing = jnp.any(
        slot_ids[:, None, None] == slot_of.reshape(row_count, top_count)[None, :, :], axis=2
    ).astype(jnp.bfloat16)
    full_down = lax.all_gather(w_down, "tp", axis=1, tiled=True)
    outgoing = jnp.dot(placing, normed, preferred_element_type=jnp.float32).astype(jnp.bfloat16)
    outgoing = outgoing.reshape(seq_size, local_experts, capacity, model_width)
    arrived = lax.all_to_all(outgoing, "sp", split_axis=0, concat_axis=0, tiled=True)
    piece = lax.all_gather(arrived, "tp", axis=0, tiled=True)
    gate_part = jnp.einsum("secd,edh->sech", piece, w_gate, preferred_element_type=jnp.float32)
    up_part = jnp.einsum("secd,edh->sech", piece, w_up, preferred_element_type=jnp.float32)
    hidden = (jax.nn.silu(gate_part) * up_part).astype(jnp.bfloat16)
    unit_rows = lax.all_to_all(hidden, "tp", split_axis=0, concat_axis=3, tiled=True)
    returned = jnp.einsum(
        "sech,ehd->secd", unit_rows, full_down, preferred_element_type=jnp.float32
    ).astype(jnp.bfloat16)
    result_rows = lax.all_to_all(returned, "sp", split_axis=0, concat_axis=0, tiled=True).reshape(
        expert_total * capacity, model_width
    )
    picked = result_rows[slot_of].astype(jnp.float32).reshape(row_count, top_count, model_width)
    return jnp.sum(picked * mixing[:, :, None], axis=1)


def swap(array, bits, tp_bits=0):
    count, width = lax.axis_size("sp"), lax.axis_size("tp")
    if tp_bits == 0:
        return lax.ppermute(array, "sp", [(s, s ^ bits) for s in range(count)])
    if bits == 0:
        return lax.ppermute(array, "tp", [(t, t ^ tp_bits) for t in range(width)])
    pairs = [
        (s * width + t, (s ^ bits) * width + (t ^ tp_bits))
        for s in range(count)
        for t in range(width)
    ]
    return lax.ppermute(array, ("sp", "tp"), pairs)


def mesh_peer(seq_bits, model_bits):
    return {"sp": lax.axis_index("sp") ^ seq_bits, "tp": lax.axis_index("tp") ^ model_bits}


def expert_kernel(
    own_ref,
    gate_ref,
    up_ref,
    down_ref,
    gate_far_ref,
    up_far_ref,
    down_far_ref,
    out_ref,
    gates,
    ups,
    downs,
    rows,
    total,
    kept,
    parts,
    landed,
    load_sems,
    weight_send,
    weight_recv,
    row_send,
    row_recv,
    part_send,
    part_recv,
):
    capacity, width = out_ref.shape[0] // 2, out_ref.shape[1]
    parity = lax.axis_index("sp") % 2
    across_y, across_x = mesh_peer(2, 0), mesh_peer(1, 0)
    across_z, sibling = mesh_peer(0, 4), mesh_peer(0, 1)

    barrier = pltpu.get_barrier_semaphore()
    for peer in (across_y, across_x, across_z, sibling):
        pl.semaphore_signal(
            barrier, inc=1, device_id=peer, device_id_type=pl.DeviceIdType.MESH
        )
    pl.semaphore_wait(barrier, 4)

    def remote(source, target, send, recv, peer):
        copy = pltpu.make_async_remote_copy(
            src_ref=source,
            dst_ref=target,
            send_sem=send,
            recv_sem=recv,
            device_id=peer,
            device_id_type=pl.DeviceIdType.MESH,
        )
        copy.start()
        return copy

    def send_rows(n, source, slot, peer):
        return remote(source, rows.at[slot], row_send.at[n], row_recv.at[slot], peer)

    def send_part(n, peer):
        return remote(parts.at[n], landed.at[n], part_send.at[n], part_recv.at[n], peer)

    sent = [
        send_rows(0, own_ref.at[1], 1, across_y),
        send_rows(1, own_ref.at[0], 2, across_x),
        send_rows(2, own_ref.at[0], 4, across_z),
    ]
    arriving = {1: sent[0], 2: sent[1], 4: sent[2]}

    weights = []
    loads = []
    holders = ((gate_ref, gates), (up_ref, ups), (down_ref, downs))
    far_holders = ((gate_far_ref, gates), (up_far_ref, ups), (down_far_ref, downs))
    for block, group in ((0, holders), (2, far_holders)):
        for n, (source, target) in enumerate(group):
            k = block // 2 * 3 + n
            load = pltpu.make_async_copy(source, target.at[block], load_sems.at[k])
            load.start()
            loads.append(load)
            weights.append(
                remote(source, target.at[block + 1], weight_send.at[k], weight_recv.at[k], sibling)
            )

    def ffn(tokens):
        mix = tokens[:, width : width + 128].astype(jnp.float32)
        scale = jnp.where(
            parity == 0, mix[:, 0:1] + mix[:, 1:2], mix[:, 2:3] + mix[:, 3:4]
        )

        def step(block, carry):
            gate_part = jnp.dot(
                tokens[:, :width], gates[block], preferred_element_type=jnp.float32
            )
            up_part = jnp.dot(tokens[:, :width], ups[block], preferred_element_type=jnp.float32)
            hidden = (gate_part / (1.0 + jnp.exp(-gate_part)) * up_part * scale).astype(
                jnp.bfloat16
            )
            part = jnp.dot(hidden, downs[block], preferred_element_type=jnp.float32)

            @pl.when(block == 0)
            def _():
                total[...] = part

            @pl.when(block > 0)
            def _():
                total[...] += part

            return carry

        lax.fori_loop(0, gates.shape[0], step, 0)

    def part_of(n, slot, peer):
        ffn(rows.at[slot])
        parts[n] = total[...].astype(jnp.bfloat16)
        return send_part(n, peer)

    arriving[1].wait_recv()
    second = [
        send_rows(3, rows.at[1], 3, across_x),
        send_rows(4, rows.at[1], 5, across_z),
    ]
    for load in loads:
        load.wait()
    for weight in weights:
        weight.wait_recv()
    arriving[2].wait_recv()
    exchanges = [part_of(0, 2, across_x)]
    arriving[4].wait_recv()
    third = send_rows(5, rows.at[4], 6, across_x)
    ffn(rows.at[4])
    kept[2] = total[...]
    second[0].wait_recv()
    exchanges.append(part_of(1, 3, across_x))
    ffn(own_ref.at[0])
    kept[0] = total[...]
    third.wait_recv()
    exchanges.append(part_of(2, 6, across_x))
    second[1].wait_recv()
    fourth = send_rows(6, rows.at[5], 7, across_x)
    ffn(rows.at[5])
    kept[3] = total[...]
    exchanges[2].wait_recv()
    parts[4] = (kept[2] + landed[2].astype(jnp.float32)).astype(jnp.bfloat16)
    hops = [send_part(4, across_z)]
    fourth.wait_recv()
    exchanges.append(part_of(3, 7, across_x))
    ffn(rows.at[1])
    kept[1] = total[...]
    exchanges[3].wait_recv()
    parts[5] = (kept[3] + landed[3].astype(jnp.float32)).astype(jnp.bfloat16)
    hops.append(send_part(5, across_z))
    exchanges[0].wait_recv()
    hops[0].wait_recv()
    out_ref[:capacity, :] = (
        kept[0] + landed[0].astype(jnp.float32) + landed[4].astype(jnp.float32)
    ).astype(jnp.bfloat16)
    exchanges[1].wait_recv()
    hops[1].wait_recv()
    parts[6] = (
        kept[1] + landed[1].astype(jnp.float32) + landed[5].astype(jnp.float32)
    ).astype(jnp.bfloat16)
    back = send_part(6, across_y)
    back.wait_recv()
    out_ref[capacity:, :] = landed[6]
    for copy in sent + second + [third, fourth] + weights + exchanges + hops + [back]:
        copy.wait_send()


def run_experts(own, near, far):
    half, capacity, wide = own.shape
    width, units = near[0].shape
    blocks = 4
    flops = 2 * 8 * capacity * blocks * units * width * 3
    whole = pl.BlockSpec(memory_space=pltpu.VMEM)
    distant = pl.BlockSpec(memory_space=pl.ANY)
    return pl.pallas_call(
        expert_kernel,
        out_shape=jax.ShapeDtypeStruct((half * capacity, width), jnp.bfloat16),
        in_specs=[whole] + [distant] * 6,
        out_specs=whole,
        scratch_shapes=[
            pltpu.VMEM((blocks, width, units), jnp.bfloat16),
            pltpu.VMEM((blocks, width, units), jnp.bfloat16),
            pltpu.VMEM((blocks, units, width), jnp.bfloat16),
            pltpu.VMEM((8, capacity, wide), jnp.bfloat16),
            pltpu.VMEM((capacity, width), jnp.float32),
            pltpu.VMEM((4, capacity, width), jnp.float32),
            pltpu.VMEM((7, capacity, width), jnp.bfloat16),
            pltpu.VMEM((7, capacity, width), jnp.bfloat16),
            pltpu.SemaphoreType.DMA((6,)),
            pltpu.SemaphoreType.DMA((6,)),
            pltpu.SemaphoreType.DMA((6,)),
            pltpu.SemaphoreType.DMA((7,)),
            pltpu.SemaphoreType.DMA((8,)),
            pltpu.SemaphoreType.DMA((7,)),
            pltpu.SemaphoreType.DMA((7,)),
        ],
        compiler_params=pltpu.CompilerParams(
            collective_id=1, has_side_effects=True, vmem_limit_bytes=48 * 1024 * 1024
        ),
        cost_estimate=pl.CostEstimate(
            flops=flops, bytes_accessed=12 * width * units * 2, transcendentals=0
        ),
        name="experts",
    )(own, *near, *far)


def routed_pairs(normed, route_experts, near, far, mixing):
    row_count, width = normed.shape
    me = lax.axis_index("sp")
    capacity = 5 * row_count // 8
    held = 2 * capacity
    group = route_experts[:, 0] // 2
    token = jnp.arange(row_count, dtype=jnp.int32)
    earlier = (group[:, None] == group[None, :]) & (token[None, :] < token[:, None])
    ordinal = jnp.sum(earlier.astype(jnp.int32), axis=1)
    slot = jnp.where(group == me // 2, 0, capacity) + ordinal
    slot_ids = jnp.arange(held, dtype=jnp.int32)
    placing = (slot_ids[:, None] == slot[None, :]).astype(jnp.bfloat16)
    shares = jnp.stack(
        [jnp.sum(jnp.where(route_experts % 2 == p, mixing, 0.0), axis=1) for p in (0, 1)], axis=1
    )
    coarse = lax.reduce_precision(shares, 8, 7)
    lane = jnp.arange(128, dtype=jnp.int32)[None, :]
    extra = jnp.zeros((row_count, 128), jnp.float32)
    for p in (0, 1):
        extra = jnp.where(lane == 2 * p, coarse[:, p : p + 1], extra)
        extra = jnp.where(lane == 2 * p + 1, (shares - coarse)[:, p : p + 1], extra)
    extended = jnp.concatenate([normed, extra.astype(jnp.bfloat16)], axis=1)
    own = jnp.dot(placing, extended, preferred_element_type=jnp.float32).astype(jnp.bfloat16)
    results = run_experts(own.reshape(2, capacity, width + 128), near, far)
    return lax.dot_general(
        placing, results, (((0,), (0,)), ((), ())), preferred_element_type=jnp.float32
    )


def local(
    queries,
    keys,
    values,
    query_gain,
    key_gain,
    out_weight,
    residual,
    norm_gain,
    route_experts,
    expert_scores,
    group_prob,
    w_gate,
    w_up,
    w_down,
):
    span_tokens = queries.shape[0]
    head_size = key_gain.shape[0]
    local_heads = queries.shape[1] // head_size
    key_heads = keys.shape[1] // head_size
    model_size = lax.axis_size("tp")
    seq_size = lax.axis_size("sp")
    share = local_heads * model_size // key_heads
    model_index = lax.axis_index("tp")
    seq_index = lax.axis_index("sp")
    local_experts = w_gate.shape[0]
    group_experts = local_experts * seq_size // GROUPS
    pairs = (
        local_experts == 1
        and GROUPS == 2
        and group_experts == 2
        and route_experts.shape[1] == 2
        and model_size == 8
    )
    halves = seq_size == 4 and model_size % 2 == 0 and share % (2 * local_heads) == 0

    cosines, sines = rope_tables(seq_index * span_tokens, span_tokens, head_size)
    shared_head = (model_index * local_heads // share).astype(jnp.int32)
    core = (model_index % 2 if halves else 0 * model_index).astype(jnp.int32)
    key_values = prep_keys(
        keys, values, key_gain, cosines, sines, jnp.stack([shared_head, core]), 2 if halves else 1
    )
    if halves:
        fetched = [key_values]
        for bits in (1, 2, 3):
            fetched.append(swap(key_values, bits))
        pieces = fetched + [swap(piece, 0, 1) for piece in fetched]
    else:
        pieces = [lax.all_gather(key_values, "sp", axis=0, tiled=True)]
    if pairs:
        near = (w_gate[0], w_up[0], w_down[0])
        far = []
        for block in near:
            far.append(swap(block, 0, 2))
    attended = attend(queries, query_gain, cosines, sines, pieces)
    all_heads = lax.all_to_all(attended, "tp", split_axis=0, concat_axis=1, tiled=True)
    update = jnp.dot(all_heads, out_weight, preferred_element_type=jnp.float32)
    updated = lax.optimization_barrier((residual.astype(jnp.float32) + update).astype(jnp.bfloat16))
    updated_wide = updated.astype(jnp.float32)
    normed = (
        updated_wide
        * lax.rsqrt(jnp.mean(updated_wide * updated_wide, axis=1, keepdims=True) + norm_eps)
        * norm_gain[None, :]
    ).astype(jnp.bfloat16)
    mixing = group_prob[:, None] * jax.nn.softmax(expert_scores, axis=1)
    if pairs:
        combined = routed_pairs(normed, route_experts, near, far, mixing)
    else:
        combined = routed_general(normed, route_experts, w_gate, w_up, w_down, mixing)
    return (updated_wide + combined).astype(jnp.bfloat16)


def solution(mesh):
    placed = (
        P("sp", "tp"),
        P("sp", None),
        P("sp", None),
        P("tp"),
        P(),
        P(),
        P(("sp", "tp"), None),
        P(),
        P(("sp", "tp"), None),
        P(("sp", "tp"), None),
        P(("sp", "tp")),
        P("sp", None, "tp"),
        P("sp", None, "tp"),
        P("sp", "tp", None),
    )
    return jax.shard_map(
        local, mesh=mesh, in_specs=placed, out_specs=P(("sp", "tp"), None), check_vma=False
    )
```

profile of v0, /device:TPU:0, one launch (start us, length us, event | category | flops | bytes accessed | tf_op | source)
XLA Modules:
  0.0 186.9 jit_solution(14964170032724494322)
XLA Ops:
  0.1 0.1 pad_maximum_fusion.1
  0.1 0.2 fusion.9
  0.4 0.7 pad_add_fusion.place_ref
  1.1 1.1 bitcast_select_fusion
  2.2 2.9 %prep_keys.1.rest_0_ = bf16[512,256]{1,0:T(8,128)(2,1)} custom-call(s32[2]{0:T(128)} %pad_add_fusion.place_ref, bf16[1024,512]{1,0:T(8,128)(2,1)} %key_ref.1, bf16[1024,512]{1,0:T(8,128)(2,1)} %value_ref.1, f32[1024,128]{1,0:T(8,128)} %get-tuple-element.16.cos_ref, f32[1024,128]{1,0:T(8,128)} %get-tuple-element.15.sin_ref, f32[1,128]{1,0:T(1,128)} %bitcast.56), custom_call_target="tpu_custom_call" | custom-call | flops 1048576 | bytes 1048576 | tf_op jit(solution)/shard_map/prep_keys/pallas_call | solution.py:77
  5.0 0.5 collective-permute-start.3
  5.5 3.4 %collective-permute-start.2 = (bf16[512,256]{1,0:T(8,128)(2,1)}, bf16[512,256]{1,0:T(8,128)(2,1)S(1)}, u32[]{:S(2)}, u32[]{:S(2)}) collective-permute-start(bf16[512,256]{1,0:T(8,128)(2,1)} %prep_keys.1.rest_0_), channel_id=1, source_target_pairs={{0,24},{8,16},{16,8},{24,0},{1,25},{9,17},{17,9},{25,1},{2,26},{10... | collective-permute-start | bytes 786440 | tf_op jit(solution)/shard_map/ppermute | solution.py:193
  8.9 0.5 collective-permute-start.1
  9.4 0.1 collective-permute-start
  9.6 2.0 %collective-permute-start.7 = (bf16[2048,256]{1,0:T(8,128)(2,1)}, bf16[2048,256]{1,0:T(8,128)(2,1)S(1)}, u32[]{:S(2)}, u32[]{:S(2)}) collective-permute-start(bf16[2048,256]{1,0:T(8,128)(2,1)} %bitcast.46), channel_id=1, source_target_pairs={{0,2},{1,3},{2,0},{3,1},{4,6},{5,7},{6,4},{7,5},{8,10},{9,11},{10,... | collective-permute-start | bytes 3145736 | tf_op jit(solution)/shard_map/ppermute | solution.py:195
  11.6 0.7 reduce_max.9
  12.3 0.7 fusion.15
  13.0 0.7 fusion.12
  13.7 0.7 fusion.22
  14.4 2.0 %collective-permute-done.2.rest_3_ = bf16[512,256]{1,0:T(8,128)(2,1)S(1)} collective-permute-done((bf16[512,256]{1,0:T(8,128)(2,1)}, bf16[512,256]{1,0:T(8,128)(2,1)S(1)}, u32[]{:S(2)}, u32[]{:S(2)}) %collective-permute-start.2) | collective-permute-done | bytes 262176 | tf_op jit(solution)/shard_map/ppermute | solution.py:193
  16.4 0.0 copy-start.8
  16.4 0.0 collective-permute-start.6
  16.4 5.4 %collective-permute-done.1.rest_2_ = bf16[512,256]{1,0:T(8,128)(2,1)S(1)} collective-permute-done((bf16[512,256]{1,0:T(8,128)(2,1)}, bf16[512,256]{1,0:T(8,128)(2,1)S(1)}, u32[]{:S(2)}, u32[]{:S(2)}) %collective-permute-start.1) | collective-permute-done | bytes 262176 | tf_op jit(solution)/shard_map/ppermute | solution.py:193
  21.7 0.0 copy-start.9
  21.7 0.0 collective-permute-start.5
  21.8 0.2 collective-permute-done.rest_1_
  22.0 0.0 copy-start.10
  22.0 0.2 collective-permute-start.4
  22.3 0.7 and_select_fusion.2
  23.0 0.0 collective-permute-done.3.rest_4_
  23.0 0.0 copy-start.7
  23.0 1.8 collective-permute-start.8
  24.8 0.0 collective-permute-done.6.rest_7_
  24.8 0.0 copy-start.11
  24.8 0.3 collective-permute-start.9
  25.1 0.0 collective-permute-done.5.rest_6_
  25.1 0.0 collective-permute-done.4.rest_5_
  25.1 0.0 copy-done.10
  25.1 0.0 copy-start.13
  25.1 0.0 copy-done.8
  25.1 0.0 copy-done.9
  25.1 0.0 copy-done.7
  25.1 0.4 copy-done.11
  25.5 0.3 copy-done.12
  25.8 0.1 copy-done.13
  25.9 29.0 %attend.1 = bf16[1024,256]{1,0:T(8,128)(2,1)} custom-call(bf16[1024,256]{1,0:T(8,128)(2,1)} %q_ref.1, f32[1024,128]{1,0:T(8,128)} %get-tuple-element.16.cos_ref, f32[1024,128]{1,0:T(8,128)} %get-tuple-element.15.sin_ref, f32[1,256]{1,0:T(1,128)} %bitcast.57, bf16[512,256]{1,0:T(8,128)(2,1)} %prep_keys.1.rest_0_, bf16[512,256]{1,0:T(8,128)(2,1)} %copy-done.10, ...), custom_call_target="tpu_custom_call" | custom-call | flops 8589934592 | bytes 4194304 | tf_op jit(solution)/shard_map/attend/pallas_call | solution.py:131
  54.9 2.0 %copy.16 = bf16[8,128,256]{1,2,0:T(8,128)(2,1)} copy(bf16[8,128,256]{2,1,0:T(8,128)(2,1)} %bitcast.53) | data formatting | bytes 1048576 | tf_op jit(solution)/shard_map/all_to_all | solution.py:492
  56.9 5.1 %all-to-all-start = ((bf16[8,128,256]{1,2,0:T(8,128)(2,1)}), bf16[8,128,256]{1,2,0:T(8,128)(2,1)S(1)}, u32[]{:S(2)}, u32[]{:S(2)}) async-start(bf16[8,128,256]{1,2,0:T(8,128)(2,1)} %copy.16), calls=%async_computation | async-start | bytes 1048576 | tf_op jit(solution)/shard_map/all_to_all | solution.py:492
  62.0 0.2 convert_reduce_fusion
  62.2 0.0 copy-done.5
  62.3 0.1 select_convert_fusion
  62.4 26.4 %all-to-all-done = bf16[8,128,256]{1,2,0:T(8,128)(2,1)S(1)} async-done(((bf16[8,128,256]{1,2,0:T(8,128)(2,1)}), bf16[8,128,256]{1,2,0:T(8,128)(2,1)S(1)}, u32[]{:S(2)}, u32[]{:S(2)}) %all-to-all-start) | async-done | bytes 524320 | tf_op jit(solution)/shard_map/all_to_all | solution.py:492
  88.8 0.0 copy-done.3
  88.8 0.0 copy-start.2
  88.8 4.8 %fusion = bf16[128,2048]{1,0:T(8,128)(2,1)S(1)} fusion(bf16[128,2048]{0,1:T(8,128)(2,1)S(1)} %bitcast.52, bf16[2048,2048]{1,0:T(8,128)(2,1)} %param.19, bf16[128,2048]{1,0:T(8,128)(2,1)S(1)} %copy-done.3), kind=kOutput, calls=%fused_computation.3 | convolution fusion | flops 1074528256 | bytes 9961472 | tf_op jit(solution)/shard_map/dot_general | solution.py:493
  93.7 0.2 fusion.2
  93.9 0.0 copy-done.4
  93.9 0.2 fusion.4
  94.1 0.3 convolution_convert_fusion
  94.4 0.0 collective-permute-done.7.gate_far_ref
  94.4 0.0 collective-permute-done.8.up_far_ref
  94.4 0.0 copy-start.6
  94.4 0.0 collective-permute-done.9.down_far_ref
  94.4 1.0 copy-done.6
  95.4 0.0 copy-done
  95.4 0.0 copy-done.1
  95.4 0.0 copy-done.2
  95.4 90.3 %experts.1 = bf16[160,2048]{1,0:T(8,128)(2,1)S(1)} custom-call(bf16[2,80,2176]{2,1,0:T(8,128)(2,1)S(1)} %bitcast.45, bf16[2048,256]{1,0:T(8,128)(2,1)S(1)} %bitcast.47, bf16[2048,256]{1,0:T(8,128)(2,1)S(1)} %bitcast.49, bf16[256,2048]{1,0:T(8,128)(2,1)S(1)} %bitcast.51, bf16[2048,256]{1,0:T(8,128)(2,1)S(1)} %collective-permute-done.7.gate_far_ref, ...), custom_call_target="tpu_custom_call" | custom-call | flops 8053063680 | bytes 12582912 | tf_op jit(solution)/shard_map/experts/pallas_call | solution.py:376
  185.8 1.1 fusion.1
  (20 shorter events, 0.1 us)
Async XLA Ops:
  5.0 17.9 %collective-permute-start.3 = (bf16[512,256]{1,0:T(8,128)(2,1)}, bf16[512,256]{1,0:T(8,128)(2,1)S(1)}, u32[]{:S(2)}, u32[]{:S(2)}) collective-permute-start(bf16[512,256]{1,0:T(8,128)(2,1)} %prep_keys.1.rest_0_), channel_id=1, source_target_pairs={{0,1},{1,0},{2,3},{3,2},{4,5},{5,4},{6,7},{7,6},{8,9},{9,8},{10,11... | collective-permute-start | bytes 786440 | tf_op jit(solution)/shard_map/ppermute | solution.py:195
  5.5 10.8 %collective-permute-start.2 = (bf16[512,256]{1,0:T(8,128)(2,1)}, bf16[512,256]{1,0:T(8,128)(2,1)S(1)}, u32[]{:S(2)}, u32[]{:S(2)}) collective-permute-start(bf16[512,256]{1,0:T(8,128)(2,1)} %prep_keys.1.rest_0_), channel_id=1, source_target_pairs={{0,24},{8,16},{16,8},{24,0},{1,25},{9,17},{17,9},{25,1},{2,26},{10... | collective-permute-start | bytes 786440 | tf_op jit(solution)/shard_map/ppermute | solution.py:193
  8.9 12.8 %collective-permute-start.1 = (bf16[512,256]{1,0:T(8,128)(2,1)}, bf16[512,256]{1,0:T(8,128)(2,1)S(1)}, u32[]{:S(2)}, u32[]{:S(2)}) collective-permute-start(bf16[512,256]{1,0:T(8,128)(2,1)} %prep_keys.1.rest_0_), channel_id=1, source_target_pairs={{0,16},{8,24},{16,0},{24,8},{1,17},{9,25},{17,1},{25,9},{2,18},{10... | collective-permute-start | bytes 786440 | tf_op jit(solution)/shard_map/ppermute | solution.py:193
  9.4 12.6 %collective-permute-start = (bf16[512,256]{1,0:T(8,128)(2,1)}, bf16[512,256]{1,0:T(8,128)(2,1)S(1)}, u32[]{:S(2)}, u32[]{:S(2)}) collective-permute-start(bf16[512,256]{1,0:T(8,128)(2,1)} %prep_keys.1.rest_0_), channel_id=1, source_target_pairs={{0,8},{8,0},{16,24},{24,16},{1,9},{9,1},{17,25},{25,17},{2,10},{10... | collective-permute-start | bytes 786440 | tf_op jit(solution)/shard_map/ppermute | solution.py:193
  9.6 84.8 %collective-permute-start.7 = (bf16[2048,256]{1,0:T(8,128)(2,1)}, bf16[2048,256]{1,0:T(8,128)(2,1)S(1)}, u32[]{:S(2)}, u32[]{:S(2)}) collective-permute-start(bf16[2048,256]{1,0:T(8,128)(2,1)} %bitcast.46), channel_id=1, source_target_pairs={{0,2},{1,3},{2,0},{3,1},{4,6},{5,7},{6,4},{7,5},{8,10},{9,11},{10,... | collective-permute-start | bytes 3145736 | tf_op jit(solution)/shard_map/ppermute | solution.py:195
  16.4 8.8 %copy-start.8 = (bf16[512,256]{1,0:T(8,128)(2,1)}, bf16[512,256]{1,0:T(8,128)(2,1)S(1)}, u32[]{:S(2)}) copy-start(bf16[512,256]{1,0:T(8,128)(2,1)S(1)} %collective-permute-done.2.rest_3_) | copy-start | bytes 786436
  16.4 8.5 %collective-permute-start.6 = (bf16[512,256]{1,0:T(8,128)(2,1)S(1)}, bf16[512,256]{1,0:T(8,128)(2,1)S(1)}, u32[]{:S(2)}, u32[]{:S(2)}) collective-permute-start(bf16[512,256]{1,0:T(8,128)(2,1)S(1)} %collective-permute-done.2.rest_3_), channel_id=1, source_target_pairs={{0,1},{1,0},{2,3},{3,2},{4,5},{5,4},{6,7},{7,6},{8,9},{9,8},{10,11... | collective-permute-start | bytes 786440 | tf_op jit(solution)/shard_map/ppermute | solution.py:195
  21.7 3.4 %copy-start.9 = (bf16[512,256]{1,0:T(8,128)(2,1)}, bf16[512,256]{1,0:T(8,128)(2,1)S(1)}, u32[]{:S(2)}) copy-start(bf16[512,256]{1,0:T(8,128)(2,1)S(1)} %collective-permute-done.1.rest_2_) | copy-start | bytes 786436
  21.7 3.3 %collective-permute-start.5 = (bf16[512,256]{1,0:T(8,128)(2,1)S(1)}, bf16[512,256]{1,0:T(8,128)(2,1)S(1)}, u32[]{:S(2)}, u32[]{:S(2)}) collective-permute-start(bf16[512,256]{1,0:T(8,128)(2,1)S(1)} %collective-permute-done.1.rest_2_), channel_id=1, source_target_pairs={{0,1},{1,0},{2,3},{3,2},{4,5},{5,4},{6,7},{7,6},{8,9},{9,8},{10,11... | collective-permute-start | bytes 786440 | tf_op jit(solution)/shard_map/ppermute | solution.py:195
  22.0 3.0 %copy-start.10 = (bf16[512,256]{1,0:T(8,128)(2,1)}, bf16[512,256]{1,0:T(8,128)(2,1)S(1)}, u32[]{:S(2)}) copy-start(bf16[512,256]{1,0:T(8,128)(2,1)S(1)} %collective-permute-done.rest_1_) | copy-start | bytes 786436
  22.0 3.0 %collective-permute-start.4 = (bf16[512,256]{1,0:T(8,128)(2,1)S(1)}, bf16[512,256]{1,0:T(8,128)(2,1)S(1)}, u32[]{:S(2)}, u32[]{:S(2)}) collective-permute-start(bf16[512,256]{1,0:T(8,128)(2,1)S(1)} %collective-permute-done.rest_1_), channel_id=1, source_target_pairs={{0,1},{1,0},{2,3},{3,2},{4,5},{5,4},{6,7},{7,6},{8,9},{9,8},{10,11... | collective-permute-start | bytes 786440 | tf_op jit(solution)/shard_map/ppermute | solution.py:195
  23.0 2.2 %copy-start.7 = (bf16[512,256]{1,0:T(8,128)(2,1)}, bf16[512,256]{1,0:T(8,128)(2,1)S(1)}, u32[]{:S(2)}) copy-start(bf16[512,256]{1,0:T(8,128)(2,1)S(1)} %collective-permute-done.3.rest_4_) | copy-start | bytes 786436
  23.0 71.4 %collective-permute-start.8 = (bf16[2048,256]{1,0:T(8,128)(2,1)}, bf16[2048,256]{1,0:T(8,128)(2,1)S(1)}, u32[]{:S(2)}, u32[]{:S(2)}) collective-permute-start(bf16[2048,256]{1,0:T(8,128)(2,1)} %bitcast.48), channel_id=1, source_target_pairs={{0,2},{1,3},{2,0},{3,1},{4,6},{5,7},{6,4},{7,5},{8,10},{9,11},{10,... | collective-permute-start | bytes 3145736 | tf_op jit(solution)/shard_map/ppermute | solution.py:195
  24.8 0.7 copy-start.11
  24.8 69.6 %collective-permute-start.9 = (bf16[256,2048]{1,0:T(8,128)(2,1)}, bf16[256,2048]{1,0:T(8,128)(2,1)}, u32[]{:S(2)}, u32[]{:S(2)}) collective-permute-start(bf16[256,2048]{1,0:T(8,128)(2,1)} %bitcast.50), channel_id=1, source_target_pairs={{0,2},{1,3},{2,0},{3,1},{4,6},{5,7},{6,4},{7,5},{8,10},{9,11},{10,... | collective-permute-start | bytes 3145736 | tf_op jit(solution)/shard_map/ppermute | solution.py:195
  25.1 0.7 copy-start.12
  25.1 0.8 copy-start.13
  25.9 36.4 %copy-start.5 = (s32[128,2]{0,1:T(2,128)S(1)}, s32[128,2]{0,1:T(2,128)}, u32[]{:S(2)}) copy-start(s32[128,2]{0,1:T(2,128)} %param.22) | copy-start | bytes 3076
  25.9 62.9 %copy-start.3 = (bf16[128,2048]{1,0:T(8,128)(2,1)S(1)}, bf16[128,2048]{1,0:T(8,128)(2,1)}, u32[]{:S(2)}) copy-start(bf16[128,2048]{1,0:T(8,128)(2,1)} %param.20) | copy-start | bytes 1572868
  56.9 31.9 %all-to-all-start = ((bf16[8,128,256]{1,2,0:T(8,128)(2,1)}), bf16[8,128,256]{1,2,0:T(8,128)(2,1)S(1)}, u32[]{:S(2)}, u32[]{:S(2)}) async-start(bf16[8,128,256]{1,2,0:T(8,128)(2,1)} %copy.16), calls=%async_computation | async-start | bytes 1048576 | tf_op jit(solution)/shard_map/all_to_all | solution.py:492
  88.8 5.0 %copy-start.4 = (f32[2048]{0:T(1024)S(1)}, f32[2048]{0:T(1024)}, u32[]{:S(2)}) copy-start(f32[2048]{0:T(1024)} %param.21) | copy-start | bytes 24580
  88.8 6.6 %copy-start = (bf16[1,2048,256]{2,1,0:T(8,128)(2,1)S(1)}, bf16[1,2048,256]{2,1,0:T(8,128)(2,1)}, u32[]{:S(2)}) copy-start(bf16[1,2048,256]{2,1,0:T(8,128)(2,1)} %param.25) | copy-start | bytes 3145732
  88.8 6.6 %copy-start.1 = (bf16[1,2048,256]{2,1,0:T(8,128)(2,1)S(1)}, bf16[1,2048,256]{2,1,0:T(8,128)(2,1)}, u32[]{:S(2)}) copy-start(bf16[1,2048,256]{2,1,0:T(8,128)(2,1)} %param.26) | copy-start | bytes 3145732
  88.8 6.6 %copy-start.2 = (bf16[1,256,2048]{2,1,0:T(8,128)(2,1)S(1)}, bf16[1,256,2048]{2,1,0:T(8,128)(2,1)}, u32[]{:S(2)}) copy-start(bf16[1,256,2048]{2,1,0:T(8,128)(2,1)} %param.27) | copy-start | bytes 3145732
  94.4 1.0 copy-start.6
where the time goes:
time: 187 us
  Pallas kernels  122 us (65%)
  waiting for transfers between devices  34 us (18%)
  starting transfers between devices  14 us (7%)
  matrix products  6.29 us (3%)
  other arithmetic  6.28 us (3%)
  local copies, waits for them, and re-layouts  3.82 us (2%)
    pallas_call x1, Pallas kernels, run_experts(): pl.pallas_call(expert_kernel, out_shape=jax.ShapeDtypeStruct((half * capa...  90.3 us
    pallas_call x1, Pallas kernels, attend(): pl.pallas_call(functools.partial(attend_kernel, len(pieces), chunk), grid...  29 us
    all_to_all x1, waiting for transfers between devices, local(): lax.all_to_all(attended, 'tp', split_axis=0, concat_axis=1, tiled=True)  26.4 us
    ppermute x3, waiting for transfers between devices, swap(): return lax.ppermute(array, 'sp', [(s, s ^ bits) for s in range(count)])  7.6 us
    all_to_all x1, starting transfers between devices, local(): lax.all_to_all(attended, 'tp', split_axis=0, concat_axis=1, tiled=True)  5.07 us
    ppermute x7, starting transfers between devices, swap(): return lax.ppermute(array, 'tp', [(t, t ^ tp_bits) for t in range(width)])  4.84 us
    dot_general x1, matrix products, local(): update = jnp.dot(all_heads, out_weight, preferred_element_type=jnp.float32)  4.82 us
    ppermute x3, starting transfers between devices, swap(): return lax.ppermute(array, 'sp', [(s, s ^ bits) for s in range(count)])  4.06 us
  transfers between devices with their start and end apart: 11, of which 4 were waited for; matrix products, arithmetic and copies ran while one was open for 6% of the time, Pallas kernels for 16%

commit v1 on v0

--- a/solution.py
+++ b/solution.py
@@ -218,7 +218,7 @@
     ups,
     downs,
     rows,
-    total,
+    hidden,
     kept,
     parts,
     landed,
@@ -231,6 +231,11 @@
     part_recv,
 ):
     capacity, width = out_ref.shape[0] // 2, out_ref.shape[1]
+    units = gate_ref.shape[1]
+    blocks = gates.shape[0]
+    first = (capacity // 2 + 15) // 16 * 16
+    pieces = (pl.ds(0, first), pl.ds(first, capacity - first))
+    full = pl.ds(0, capacity)
     parity = lax.axis_index("sp") % 2
     across_y, across_x = mesh_peer(2, 0), mesh_peer(1, 0)
     across_z, sibling = mesh_peer(0, 4), mesh_peer(0, 1)
@@ -241,6 +246,8 @@
             barrier, inc=1, device_id=peer, device_id_type=pl.DeviceIdType.MESH
         )
     pl.semaphore_wait(barrier, 4)
+
+    started = []
 
     def remote(source, target, send, recv, peer):
         copy = pltpu.make_async_remote_copy(
@@ -252,20 +259,30 @@
             device_id_type=pl.DeviceIdType.MESH,
         )
         copy.start()
+        started.append(copy)
         return copy
 
-    def send_rows(n, source, slot, peer):
-        return remote(source, rows.at[slot], row_send.at[n], row_recv.at[slot], peer)
-
-    def send_part(n, peer):
-        return remote(parts.at[n], landed.at[n], part_send.at[n], part_recv.at[n], peer)
-
-    sent = [
-        send_rows(0, own_ref.at[1], 1, across_y),
-        send_rows(1, own_ref.at[0], 2, across_x),
-        send_rows(2, own_ref.at[0], 4, across_z),
-    ]
-    arriving = {1: sent[0], 2: sent[1], 4: sent[2]}
+    def send_rows(source, slot, p, span, peer):
+        return remote(
+            source.at[span],
+            rows.at[slot, span],
+            row_send.at[slot, p],
+            row_recv.at[slot, p],
+            peer,
+        )
+
+    def send_part(n, p, span, peer):
+        return remote(
+            parts.at[n, span],
+            landed.at[n, span],
+            part_send.at[n, p],
+            part_recv.at[n, p],
+            peer,
+        )
+
+    over_y = [send_rows(own_ref.at[1], 1, p, pieces[p], across_y) for p in (0, 1)]
+    over_x = send_rows(own_ref.at[0], 2, 0, full, across_x)
+    over_z = [send_rows(own_ref.at[0], 4, p, pieces[p], across_z) for p in (0, 1)]
 
     weights = []
     loads = []
@@ -281,88 +298,118 @@
                 remote(source, target.at[block + 1], weight_send.at[k], weight_recv.at[k], sibling)
             )
 
-    def ffn(tokens):
+    def ffn(tokens, put):
+        count = tokens.shape[0]
         mix = tokens[:, width : width + 128].astype(jnp.float32)
         scale = jnp.where(
             parity == 0, mix[:, 0:1] + mix[:, 1:2], mix[:, 2:3] + mix[:, 3:4]
         )
-
-        def step(block, carry):
+        for block in range(blocks):
             gate_part = jnp.dot(
                 tokens[:, :width], gates[block], preferred_element_type=jnp.float32
             )
             up_part = jnp.dot(tokens[:, :width], ups[block], preferred_element_type=jnp.float32)
-            hidden = (gate_part / (1.0 + jnp.exp(-gate_part)) * up_part * scale).astype(
-                jnp.bfloat16
-            )
-            part = jnp.dot(hidden, downs[block], preferred_element_type=jnp.float32)
-
-            @pl.when(block == 0)
-            def _():
-                total[...] = part
-
-            @pl.when(block > 0)
-            def _():
-                total[...] += part
-
-            return carry
-
-        lax.fori_loop(0, gates.shape[0], step, 0)
-
-    def part_of(n, slot, peer):
-        ffn(rows.at[slot])
-        parts[n] = total[...].astype(jnp.bfloat16)
-        return send_part(n, peer)
-
-    arriving[1].wait_recv()
-    second = [
-        send_rows(3, rows.at[1], 3, across_x),
-        send_rows(4, rows.at[1], 5, across_z),
-    ]
+            hidden[:count, block * units : (block + 1) * units] = (
+                gate_part / (1.0 + jnp.exp(-gate_part)) * up_part * scale
+            ).astype(jnp.bfloat16)
+        for start in range(0, width, 2 * units):
+            columns = slice(start, start + 2 * units)
+            total = None
+            for block in range(blocks):
+                part = jnp.dot(
+                    hidden[:count, block * units : (block + 1) * units],
+                    downs[block, :, columns],
+                    preferred_element_type=jnp.float32,
+                )
+                total = part if total is None else total + part
+            put(columns, total)
+
+    def keep(n, tokens):
+        def put(columns, total):
+            kept[n, :, columns] = total
+
+        ffn(tokens, put)
+
+    def part_of(n, tokens, span):
+        def put(columns, total):
+            parts[n, span, columns] = total.astype(jnp.bfloat16)
+
+        ffn(tokens, put)
+
+    def hop(n, p):
+        span = pieces[p]
+        parts[4 + n, span] = (
+            kept[2 + n, span] + landed[2 + n, span].astype(jnp.float32)
+        ).astype(jnp.bfloat16)
+        return send_part(4 + n, p, span, across_z)
+
+    def settled(n, span):
+        return (
+            kept[n, span] + landed[n, span].astype(jnp.float32)
+            + landed[4 + n, span].astype(jnp.float32)
+        ).astype(jnp.bfloat16)
+
+    over_x_far, over_z_far = [], []
+    for p in (0, 1):
+        over_y[p].wait_recv()
+        over_x_far.append(send_rows(rows.at[1], 3, p, pieces[p], across_x))
+        over_z_far.append(send_rows(rows.at[1], 5, p, pieces[p], across_z))
+    over_z[0].wait_recv()
+    passed = [send_rows(rows.at[4], 6, 0, pieces[0], across_x)]
     for load in loads:
         load.wait()
     for weight in weights:
         weight.wait_recv()
-    arriving[2].wait_recv()
-    exchanges = [part_of(0, 2, across_x)]
-    arriving[4].wait_recv()
-    third = send_rows(5, rows.at[4], 6, across_x)
-    ffn(rows.at[4])
-    kept[2] = total[...]
-    second[0].wait_recv()
-    exchanges.append(part_of(1, 3, across_x))
-    ffn(own_ref.at[0])
-    kept[0] = total[...]
-    third.wait_recv()
-    exchanges.append(part_of(2, 6, across_x))
-    second[1].wait_recv()
-    fourth = send_rows(6, rows.at[5], 7, across_x)
-    ffn(rows.at[5])
-    kept[3] = total[...]
-    exchanges[2].wait_recv()
-    parts[4] = (kept[2] + landed[2].astype(jnp.float32)).astype(jnp.bfloat16)
-    hops = [send_part(4, across_z)]
-    fourth.wait_recv()
-    exchanges.append(part_of(3, 7, across_x))
-    ffn(rows.at[1])
-    kept[1] = total[...]
-    exchanges[3].wait_recv()
-    parts[5] = (kept[3] + landed[3].astype(jnp.float32)).astype(jnp.bfloat16)
-    hops.append(send_part(5, across_z))
-    exchanges[0].wait_recv()
-    hops[0].wait_recv()
-    out_ref[:capacity, :] = (
-        kept[0] + landed[0].astype(jnp.float32) + landed[4].astype(jnp.float32)
-    ).astype(jnp.bfloat16)
-    exchanges[1].wait_recv()
-    hops[1].wait_recv()
-    parts[6] = (
-        kept[1] + landed[1].astype(jnp.float32) + landed[5].astype(jnp.float32)
-    ).astype(jnp.bfloat16)
-    back = send_part(6, across_y)
-    back.wait_recv()
+    keep(0, own_ref.at[0])
+    over_z[1].wait_recv()
+    passed.append(send_rows(rows.at[4], 6, 1, pieces[1], across_x))
+    keep(2, rows.at[4])
+    exchanged = []
+    for p in (0, 1):
+        passed[p].wait_recv()
+        part_of(2, rows.at[6, pieces[p]], pieces[p])
+        exchanged.append(send_part(2, p, pieces[p], across_x))
+    over_z_far[0].wait_recv()
+    passed_far = [send_rows(rows.at[5], 7, 0, pieces[0], across_x)]
+    keep(1, rows.at[1])
+    exchanged[0].wait_recv()
+    hops = [hop(0, 0)]
+    over_z_far[1].wait_recv()
+    passed_far.append(send_rows(rows.at[5], 7, 1, pieces[1], across_x))
+    keep(3, rows.at[5])
+    passed_far[0].wait_recv()
+    part_of(3, rows.at[7, pieces[0]], pieces[0])
+    exchanged_far = [send_part(3, 0, pieces[0], across_x)]
+    exchanged[1].wait_recv()
+    hops.append(hop(0, 1))
+    passed_far[1].wait_recv()
+    part_of(3, rows.at[7, pieces[1]], pieces[1])
+    exchanged_far.append(send_part(3, 1, pieces[1], across_x))
+    exchanged_far[0].wait_recv()
+    hops_far = [hop(1, 0)]
+    for p in (0, 1):
+        over_x_far[p].wait_recv()
+    part_of(1, rows.at[3], full)
+    direct_far = [send_part(1, p, pieces[p], across_x) for p in (0, 1)]
+    exchanged_far[1].wait_recv()
+    hops_far.append(hop(1, 1))
+    over_x.wait_recv()
+    part_of(0, rows.at[2], full)
+    direct = send_part(0, 0, full, across_x)
+    back = []
+    for p in (0, 1):
+        direct_far[p].wait_recv()
+        hops_far[p].wait_recv()
+        parts[6, pieces[p]] = settled(1, pieces[p])
+        back.append(send_part(6, p, pieces[p], across_y))
+    direct.wait_recv()
+    for copy in hops:
+        copy.wait_recv()
+    out_ref[:capacity, :] = settled(0, full)
+    for copy in back:
+        copy.wait_recv()
     out_ref[capacity:, :] = landed[6]
-    for copy in sent + second + [third, fourth] + weights + exchanges + hops + [back]:
+    for copy in started:
         copy.wait_send()
 
 
@@ -383,17 +430,17 @@
             pltpu.VMEM((blocks, width, units), jnp.bfloat16),
             pltpu.VMEM((blocks, units, width), jnp.bfloat16),
             pltpu.VMEM((8, capacity, wide), jnp.bfloat16),
-            pltpu.VMEM((capacity, width), jnp.float32),
+            pltpu.VMEM((capacity, blocks * units), jnp.bfloat16),
             pltpu.VMEM((4, capacity, width), jnp.float32),
             pltpu.VMEM((7, capacity, width), jnp.bfloat16),
             pltpu.VMEM((7, capacity, width), jnp.bfloat16),
             pltpu.SemaphoreType.DMA((6,)),
             pltpu.SemaphoreType.DMA((6,)),
             pltpu.SemaphoreType.DMA((6,)),
-            pltpu.SemaphoreType.DMA((7,)),
-            pltpu.SemaphoreType.DMA((8,)),
-            pltpu.SemaphoreType.DMA((7,)),
-            pltpu.SemaphoreType.DMA((7,)),
+            pltpu.SemaphoreType.DMA((8, 2)),
+            pltpu.SemaphoreType.DMA((8, 2)),
+            pltpu.SemaphoreType.DMA((7, 2)),
+            pltpu.SemaphoreType.DMA((7, 2)),
         ],
         compiler_params=pltpu.CompilerParams(
             collective_id=1, has_side_effects=True, vmem_limit_bytes=48 * 1024 * 1024
@@ -473,8 +520,19 @@
     cosines, sines = rope_tables(seq_index * span_tokens, span_tokens, head_size)
     shared_head = (model_index * local_heads // share).astype(jnp.int32)
     core = (model_index % 2 if halves else 0 * model_index).astype(jnp.int32)
+    if pairs:
+        near = (w_gate[0], w_up[0], w_down[0])
+        far = []
+        for block in near:
+            far.append(swap(block, 0, 2))
     key_values = prep_keys(
-        keys, values, key_gain, cosines, sines, jnp.stack([shared_head, core]), 2 if halves else 1
+        keys,
+        values,
+        key_gain,
+        cosines,
+        sines,
+        jnp.stack([shared_head, core]),
+        2 if halves else 1,
     )
     if halves:
         fetched = [key_values]
@@ -483,11 +541,6 @@
         pieces = fetched + [swap(piece, 0, 1) for piece in fetched]
     else:
         pieces = [lax.all_gather(key_values, "sp", axis=0, tiled=True)]
-    if pairs:
-        near = (w_gate[0], w_up[0], w_down[0])
-        far = []
-        for block in near:
-            far.append(swap(block, 0, 2))
     attended = attend(queries, query_gain, cosines, sines, pieces)
     all_heads = lax.all_to_all(attended, "tp", split_axis=0, concat_axis=1, tiled=True)
     update = jnp.dot(all_heads, out_weight, preferred_element_type=jnp.float32)

time: 187 us -> 167 us (0.89)
  Pallas kernels: 122 us -> 102 us
    pallas_call x1, Pallas kernels: 90.3 us -> 69.7 us  [run_experts(): pl.pallas_call(expert_kernel, out_shape=jax.ShapeDtypeStruct((half * capa...]
  transfers between devices with their start and end apart: 11 -> 11, of which waited for: 4 -> 4; matrix products, arithmetic and copies ran while one was open for 6% -> 7% of each run, Pallas kernels for 16% -> 17%
where the time goes in v1:
time: 167 us; the launch traced here: 166 us
  Pallas kernels  102 us (61%)
  waiting for transfers between devices  34 us (20%)
  starting transfers between devices  14 us (8%)
  matrix products  6.29 us (4%)
  other arithmetic  6.28 us (4%)
  local copies, waits for them, and re-layouts  3.82 us (2%)
    pallas_call x1, Pallas kernels, run_experts(): pl.pallas_call(expert_kernel, out_shape=jax.ShapeDtypeStruct((half * capa...  69.7 us
    pallas_call x1, Pallas kernels, attend(): pl.pallas_call(functools.partial(attend_kernel, len(pieces), chunk), grid...  29 us
    all_to_all x1, waiting for transfers between devices, local(): lax.all_to_all(attended, 'tp', split_axis=0, concat_axis=1, tiled=True)  26.4 us
    ppermute x3, waiting for transfers between devices, swap(): return lax.ppermute(array, 'sp', [(s, s ^ bits) for s in range(count)])  7.6 us
    all_to_all x1, starting transfers between devices, local(): lax.all_to_all(attended, 'tp', split_axis=0, concat_axis=1, tiled=True)  5.07 us
    ppermute x7, starting transfers between devices, swap(): return lax.ppermute(array, 'tp', [(t, t ^ tp_bits) for t in range(width)])  4.84 us
    dot_general x1, matrix products, local(): update = jnp.dot(all_heads, out_weight, preferred_element_type=jnp.float32)  4.82 us
    ppermute x3, starting transfers between devices, swap(): return lax.ppermute(array, 'sp', [(s, s ^ bits) for s in range(count)])  4.06 us
  transfers between devices with their start and end apart: 11, of which 4 were waited for; matrix products, arithmetic and copies ran while one was open for 7% of the time, Pallas kernels for 17%

profile of v1, /device:TPU:0, one launch (start us, length us, event | category | flops | bytes accessed | tf_op | source)
XLA Modules:
  0.0 166.3 jit_solution(10745883646624539871)
XLA Ops:
  0.1 0.1 pad_maximum_fusion.1
  0.1 0.2 fusion.9
  0.4 0.7 pad_add_fusion.place_ref
  1.1 1.1 bitcast_select_fusion
  2.2 2.9 %prep_keys.1.rest_0_ = bf16[512,256]{1,0:T(8,128)(2,1)} custom-call(s32[2]{0:T(128)} %pad_add_fusion.place_ref, bf16[1024,512]{1,0:T(8,128)(2,1)} %key_ref.1, bf16[1024,512]{1,0:T(8,128)(2,1)} %value_ref.1, f32[1024,128]{1,0:T(8,128)} %get-tuple-element.16.cos_ref, f32[1024,128]{1,0:T(8,128)} %get-tuple-element.15.sin_ref, f32[1,128]{1,0:T(1,128)} %bitcast.56), custom_call_target="tpu_custom_call" | custom-call | flops 1048576 | bytes 1048576 | tf_op jit(solution)/shard_map/prep_keys/pallas_call | solution.py:77
  5.0 0.5 collective-permute-start.3
  5.5 3.4 %collective-permute-start.2 = (bf16[512,256]{1,0:T(8,128)(2,1)}, bf16[512,256]{1,0:T(8,128)(2,1)S(1)}, u32[]{:S(2)}, u32[]{:S(2)}) collective-permute-start(bf16[512,256]{1,0:T(8,128)(2,1)} %prep_keys.1.rest_0_), channel_id=1, source_target_pairs={{0,24},{8,16},{16,8},{24,0},{1,25},{9,17},{17,9},{25,1},{2,26},{10... | collective-permute-start | bytes 786440 | tf_op jit(solution)/shard_map/ppermute | solution.py:193
  8.9 0.5 collective-permute-start.1
  9.4 0.1 collective-permute-start
  9.6 2.0 %collective-permute-start.7 = (bf16[2048,256]{1,0:T(8,128)(2,1)}, bf16[2048,256]{1,0:T(8,128)(2,1)S(1)}, u32[]{:S(2)}, u32[]{:S(2)}) collective-permute-start(bf16[2048,256]{1,0:T(8,128)(2,1)} %bitcast.46), channel_id=1, source_target_pairs={{0,2},{1,3},{2,0},{3,1},{4,6},{5,7},{6,4},{7,5},{8,10},{9,11},{10,... | collective-permute-start | bytes 3145736 | tf_op jit(solution)/shard_map/ppermute | solution.py:195
  11.6 0.7 reduce_max.9
  12.3 0.7 fusion.15
  13.0 0.7 fusion.12
  13.7 0.7 fusion.22
  14.4 2.0 %collective-permute-done.2.rest_3_ = bf16[512,256]{1,0:T(8,128)(2,1)S(1)} collective-permute-done((bf16[512,256]{1,0:T(8,128)(2,1)}, bf16[512,256]{1,0:T(8,128)(2,1)S(1)}, u32[]{:S(2)}, u32[]{:S(2)}) %collective-permute-start.2) | collective-permute-done | bytes 262176 | tf_op jit(solution)/shard_map/ppermute | solution.py:193
  16.4 0.0 copy-start.8
  16.4 0.0 collective-permute-start.6
  16.4 5.4 %collective-permute-done.1.rest_2_ = bf16[512,256]{1,0:T(8,128)(2,1)S(1)} collective-permute-done((bf16[512,256]{1,0:T(8,128)(2,1)}, bf16[512,256]{1,0:T(8,128)(2,1)S(1)}, u32[]{:S(2)}, u32[]{:S(2)}) %collective-permute-start.1) | collective-permute-done | bytes 262176 | tf_op jit(solution)/shard_map/ppermute | solution.py:193
  21.7 0.0 copy-start.9
  21.7 0.0 collective-permute-start.5
  21.8 0.2 collective-permute-done.rest_1_
  22.0 0.0 copy-start.10
  22.0 0.2 collective-permute-start.4
  22.3 0.7 and_select_fusion.2
  23.0 0.0 collective-permute-done.3.rest_4_
  23.0 0.0 copy-start.7
  23.0 1.8 %collective-permute-start.8 = (bf16[2048,256]{1,0:T(8,128)(2,1)}, bf16[2048,256]{1,0:T(8,128)(2,1)S(1)}, u32[]{:S(2)}, u32[]{:S(2)}) collective-permute-start(bf16[2048,256]{1,0:T(8,128)(2,1)} %bitcast.48), channel_id=1, source_target_pairs={{0,2},{1,3},{2,0},{3,1},{4,6},{5,7},{6,4},{7,5},{8,10},{9,11},{10,... | collective-permute-start | bytes 3145736 | tf_op jit(solution)/shard_map/ppermute | solution.py:195
  24.8 0.0 collective-permute-done.6.rest_7_
  24.8 0.0 copy-start.11
  24.8 0.3 collective-permute-start.9
  25.1 0.0 collective-permute-done.5.rest_6_
  25.1 0.0 collective-permute-done.4.rest_5_
  25.1 0.0 copy-done.10
  25.1 0.0 copy-start.13
  25.1 0.0 copy-done.8
  25.1 0.0 copy-done.9
  25.1 0.0 copy-done.7
  25.1 0.4 copy-done.11
  25.5 0.3 copy-done.12
  25.8 0.1 copy-done.13
  25.9 29.0 %attend.1 = bf16[1024,256]{1,0:T(8,128)(2,1)} custom-call(bf16[1024,256]{1,0:T(8,128)(2,1)} %q_ref.1, f32[1024,128]{1,0:T(8,128)} %get-tuple-element.16.cos_ref, f32[1024,128]{1,0:T(8,128)} %get-tuple-element.15.sin_ref, f32[1,256]{1,0:T(1,128)} %bitcast.57, bf16[512,256]{1,0:T(8,128)(2,1)} %prep_keys.1.rest_0_, bf16[512,256]{1,0:T(8,128)(2,1)} %copy-done.10, ...), custom_call_target="tpu_custom_call" | custom-call | flops 8589934592 | bytes 4194304 | tf_op jit(solution)/shard_map/attend/pallas_call | solution.py:131
  54.9 2.0 %copy.16 = bf16[8,128,256]{1,2,0:T(8,128)(2,1)} copy(bf16[8,128,256]{2,1,0:T(8,128)(2,1)} %bitcast.53) | data formatting | bytes 1048576 | tf_op jit(solution)/shard_map/all_to_all | solution.py:545
  56.9 5.1 %all-to-all-start = ((bf16[8,128,256]{1,2,0:T(8,128)(2,1)}), bf16[8,128,256]{1,2,0:T(8,128)(2,1)S(1)}, u32[]{:S(2)}, u32[]{:S(2)}) async-start(bf16[8,128,256]{1,2,0:T(8,128)(2,1)} %copy.16), calls=%async_computation | async-start | bytes 1048576 | tf_op jit(solution)/shard_map/all_to_all | solution.py:545
  62.0 0.2 convert_reduce_fusion
  62.2 0.0 copy-done.5
  62.3 0.1 select_convert_fusion
  62.4 26.4 %all-to-all-done = bf16[8,128,256]{1,2,0:T(8,128)(2,1)S(1)} async-done(((bf16[8,128,256]{1,2,0:T(8,128)(2,1)}), bf16[8,128,256]{1,2,0:T(8,128)(2,1)S(1)}, u32[]{:S(2)}, u32[]{:S(2)}) %all-to-all-start) | async-done | bytes 524320 | tf_op jit(solution)/shard_map/all_to_all | solution.py:545
  88.8 0.0 copy-done.3
  88.8 0.0 copy-start.2
  88.8 4.8 %fusion = bf16[128,2048]{1,0:T(8,128)(2,1)S(1)} fusion(bf16[128,2048]{0,1:T(8,128)(2,1)S(1)} %bitcast.52, bf16[2048,2048]{1,0:T(8,128)(2,1)} %param.19, bf16[128,2048]{1,0:T(8,128)(2,1)S(1)} %copy-done.3), kind=kOutput, calls=%fused_computation.3 | convolution fusion | flops 1074528256 | bytes 9961472 | tf_op jit(solution)/shard_map/dot_general | solution.py:546
  93.7 0.2 fusion.2
  93.9 0.0 copy-done.4
  93.9 0.2 fusion.4
  94.1 0.3 convolution_convert_fusion
  94.4 0.0 collective-permute-done.7.gate_far_ref
  94.4 0.0 collective-permute-done.8.up_far_ref
  94.4 0.0 copy-start.6
  94.4 0.0 collective-permute-done.9.down_far_ref
  94.4 1.0 copy-done.6
  95.4 0.0 copy-done
  95.4 0.0 copy-done.1
  95.4 0.0 copy-done.2
  95.4 69.7 %experts.1 = bf16[160,2048]{1,0:T(8,128)(2,1)S(1)} custom-call(bf16[2,80,2176]{2,1,0:T(8,128)(2,1)S(1)} %bitcast.45, bf16[2048,256]{1,0:T(8,128)(2,1)S(1)} %bitcast.47, bf16[2048,256]{1,0:T(8,128)(2,1)S(1)} %bitcast.49, bf16[256,2048]{1,0:T(8,128)(2,1)S(1)} %bitcast.51, bf16[2048,256]{1,0:T(8,128)(2,1)S(1)} %collective-permute-done.7.gate_far_ref, ...), custom_call_target="tpu_custom_call" | custom-call | flops 8053063680 | bytes 12582912 | tf_op jit(solution)/shard_map/experts/pallas_call | solution.py:423
  165.1 1.1 fusion.1
  (20 shorter events, 0.1 us)
Async XLA Ops:
  5.0 17.9 %collective-permute-start.3 = (bf16[512,256]{1,0:T(8,128)(2,1)}, bf16[512,256]{1,0:T(8,128)(2,1)S(1)}, u32[]{:S(2)}, u32[]{:S(2)}) collective-permute-start(bf16[512,256]{1,0:T(8,128)(2,1)} %prep_keys.1.rest_0_), channel_id=1, source_target_pairs={{0,1},{1,0},{2,3},{3,2},{4,5},{5,4},{6,7},{7,6},{8,9},{9,8},{10,11... | collective-permute-start | bytes 786440 | tf_op jit(solution)/shard_map/ppermute | solution.py:195
  5.5 10.8 %collective-permute-start.2 = (bf16[512,256]{1,0:T(8,128)(2,1)}, bf16[512,256]{1,0:T(8,128)(2,1)S(1)}, u32[]{:S(2)}, u32[]{:S(2)}) collective-permute-start(bf16[512,256]{1,0:T(8,128)(2,1)} %prep_keys.1.rest_0_), channel_id=1, source_target_pairs={{0,24},{8,16},{16,8},{24,0},{1,25},{9,17},{17,9},{25,1},{2,26},{10... | collective-permute-start | bytes 786440 | tf_op jit(solution)/shard_map/ppermute | solution.py:193
  8.9 12.8 %collective-permute-start.1 = (bf16[512,256]{1,0:T(8,128)(2,1)}, bf16[512,256]{1,0:T(8,128)(2,1)S(1)}, u32[]{:S(2)}, u32[]{:S(2)}) collective-permute-start(bf16[512,256]{1,0:T(8,128)(2,1)} %prep_keys.1.rest_0_), channel_id=1, source_target_pairs={{0,16},{8,24},{16,0},{24,8},{1,17},{9,25},{17,1},{25,9},{2,18},{10... | collective-permute-start | bytes 786440 | tf_op jit(solution)/shard_map/ppermute | solution.py:193
  9.4 12.6 %collective-permute-start = (bf16[512,256]{1,0:T(8,128)(2,1)}, bf16[512,256]{1,0:T(8,128)(2,1)S(1)}, u32[]{:S(2)}, u32[]{:S(2)}) collective-permute-start(bf16[512,256]{1,0:T(8,128)(2,1)} %prep_keys.1.rest_0_), channel_id=1, source_target_pairs={{0,8},{8,0},{16,24},{24,16},{1,9},{9,1},{17,25},{25,17},{2,10},{10... | collective-permute-start | bytes 786440 | tf_op jit(solution)/shard_map/ppermute | solution.py:193
  9.6 84.8 %collective-permute-start.7 = (bf16[2048,256]{1,0:T(8,128)(2,1)}, bf16[2048,256]{1,0:T(8,128)(2,1)S(1)}, u32[]{:S(2)}, u32[]{:S(2)}) collective-permute-start(bf16[2048,256]{1,0:T(8,128)(2,1)} %bitcast.46), channel_id=1, source_target_pairs={{0,2},{1,3},{2,0},{3,1},{4,6},{5,7},{6,4},{7,5},{8,10},{9,11},{10,... | collective-permute-start | bytes 3145736 | tf_op jit(solution)/shard_map/ppermute | solution.py:195
  16.4 8.8 %copy-start.8 = (bf16[512,256]{1,0:T(8,128)(2,1)}, bf16[512,256]{1,0:T(8,128)(2,1)S(1)}, u32[]{:S(2)}) copy-start(bf16[512,256]{1,0:T(8,128)(2,1)S(1)} %collective-permute-done.2.rest_3_) | copy-start | bytes 786436
  16.4 8.5 %collective-permute-start.6 = (bf16[512,256]{1,0:T(8,128)(2,1)S(1)}, bf16[512,256]{1,0:T(8,128)(2,1)S(1)}, u32[]{:S(2)}, u32[]{:S(2)}) collective-permute-start(bf16[512,256]{1,0:T(8,128)(2,1)S(1)} %collective-permute-done.2.rest_3_), channel_id=1, source_target_pairs={{0,1},{1,0},{2,3},{3,2},{4,5},{5,4},{6,7},{7,6},{8,9},{9,8},{10,11... | collective-permute-start | bytes 786440 | tf_op jit(solution)/shard_map/ppermute | solution.py:195
  21.7 3.4 %copy-start.9 = (bf16[512,256]{1,0:T(8,128)(2,1)}, bf16[512,256]{1,0:T(8,128)(2,1)S(1)}, u32[]{:S(2)}) copy-start(bf16[512,256]{1,0:T(8,128)(2,1)S(1)} %collective-permute-done.1.rest_2_) | copy-start | bytes 786436
  21.7 3.3 %collective-permute-start.5 = (bf16[512,256]{1,0:T(8,128)(2,1)S(1)}, bf16[512,256]{1,0:T(8,128)(2,1)S(1)}, u32[]{:S(2)}, u32[]{:S(2)}) collective-permute-start(bf16[512,256]{1,0:T(8,128)(2,1)S(1)} %collective-permute-done.1.rest_2_), channel_id=1, source_target_pairs={{0,1},{1,0},{2,3},{3,2},{4,5},{5,4},{6,7},{7,6},{8,9},{9,8},{10,11... | collective-permute-start | bytes 786440 | tf_op jit(solution)/shard_map/ppermute | solution.py:195
  22.0 3.0 %copy-start.10 = (bf16[512,256]{1,0:T(8,128)(2,1)}, bf16[512,256]{1,0:T(8,128)(2,1)S(1)}, u32[]{:S(2)}) copy-start(bf16[512,256]{1,0:T(8,128)(2,1)S(1)} %collective-permute-done.rest_1_) | copy-start | bytes 786436
  22.0 3.0 %collective-permute-start.4 = (bf16[512,256]{1,0:T(8,128)(2,1)S(1)}, bf16[512,256]{1,0:T(8,128)(2,1)S(1)}, u32[]{:S(2)}, u32[]{:S(2)}) collective-permute-start(bf16[512,256]{1,0:T(8,128)(2,1)S(1)} %collective-permute-done.rest_1_), channel_id=1, source_target_pairs={{0,1},{1,0},{2,3},{3,2},{4,5},{5,4},{6,7},{7,6},{8,9},{9,8},{10,11... | collective-permute-start | bytes 786440 | tf_op jit(solution)/shard_map/ppermute | solution.py:195
  23.0 2.2 %copy-start.7 = (bf16[512,256]{1,0:T(8,128)(2,1)}, bf16[512,256]{1,0:T(8,128)(2,1)S(1)}, u32[]{:S(2)}) copy-start(bf16[512,256]{1,0:T(8,128)(2,1)S(1)} %collective-permute-done.3.rest_4_) | copy-start | bytes 786436
  23.0 71.4 %collective-permute-start.8 = (bf16[2048,256]{1,0:T(8,128)(2,1)}, bf16[2048,256]{1,0:T(8,128)(2,1)S(1)}, u32[]{:S(2)}, u32[]{:S(2)}) collective-permute-start(bf16[2048,256]{1,0:T(8,128)(2,1)} %bitcast.48), channel_id=1, source_target_pairs={{0,2},{1,3},{2,0},{3,1},{4,6},{5,7},{6,4},{7,5},{8,10},{9,11},{10,... | collective-permute-start | bytes 3145736 | tf_op jit(solution)/shard_map/ppermute | solution.py:195
  24.8 0.7 copy-start.11
  24.8 69.6 %collective-permute-start.9 = (bf16[256,2048]{1,0:T(8,128)(2,1)}, bf16[256,2048]{1,0:T(8,128)(2,1)}, u32[]{:S(2)}, u32[]{:S(2)}) collective-permute-start(bf16[256,2048]{1,0:T(8,128)(2,1)} %bitcast.50), channel_id=1, source_target_pairs={{0,2},{1,3},{2,0},{3,1},{4,6},{5,7},{6,4},{7,5},{8,10},{9,11},{10,... | collective-permute-start | bytes 3145736 | tf_op jit(solution)/shard_map/ppermute | solution.py:195
  25.1 0.7 copy-start.12
  25.1 0.8 copy-start.13
  25.9 36.4 %copy-start.5 = (s32[128,2]{0,1:T(2,128)S(1)}, s32[128,2]{0,1:T(2,128)}, u32[]{:S(2)}) copy-start(s32[128,2]{0,1:T(2,128)} %param.22) | copy-start | bytes 3076
  25.9 62.9 %copy-start.3 = (bf16[128,2048]{1,0:T(8,128)(2,1)S(1)}, bf16[128,2048]{1,0:T(8,128)(2,1)}, u32[]{:S(2)}) copy-start(bf16[128,2048]{1,0:T(8,128)(2,1)} %param.20) | copy-start | bytes 1572868
  56.9 31.9 %all-to-all-start = ((bf16[8,128,256]{1,2,0:T(8,128)(2,1)}), bf16[8,128,256]{1,2,0:T(8,128)(2,1)S(1)}, u32[]{:S(2)}, u32[]{:S(2)}) async-start(bf16[8,128,256]{1,2,0:T(8,128)(2,1)} %copy.16), calls=%async_computation | async-start | bytes 1048576 | tf_op jit(solution)/shard_map/all_to_all | solution.py:545
  88.8 5.0 %copy-start.4 = (f32[2048]{0:T(1024)S(1)}, f32[2048]{0:T(1024)}, u32[]{:S(2)}) copy-start(f32[2048]{0:T(1024)} %param.21) | copy-start | bytes 24580
  88.8 6.6 %copy-start = (bf16[1,2048,256]{2,1,0:T(8,128)(2,1)S(1)}, bf16[1,2048,256]{2,1,0:T(8,128)(2,1)}, u32[]{:S(2)}) copy-start(bf16[1,2048,256]{2,1,0:T(8,128)(2,1)} %param.25) | copy-start | bytes 3145732
  88.8 6.6 %copy-start.1 = (bf16[1,2048,256]{2,1,0:T(8,128)(2,1)S(1)}, bf16[1,2048,256]{2,1,0:T(8,128)(2,1)}, u32[]{:S(2)}) copy-start(bf16[1,2048,256]{2,1,0:T(8,128)(2,1)} %param.26) | copy-start | bytes 3145732
  88.8 6.6 %copy-start.2 = (bf16[1,256,2048]{2,1,0:T(8,128)(2,1)S(1)}, bf16[1,256,2048]{2,1,0:T(8,128)(2,1)}, u32[]{:S(2)}) copy-start(bf16[1,256,2048]{2,1,0:T(8,128)(2,1)} %param.27) | copy-start | bytes 3145732
  94.4 1.0 copy-start.6
